TPU v7x, 128 devices: a whole 4x4x4 slice. The times are simulated.
128 devices in a mesh: sp: 16 (over z, y), tp: 8 (over x, core).
Axes of the slice: x: 4, y: 4, z: 4, core: 2. Of those that a mesh axis runs over, the one named last changes fastest.
Arguments:
- inputs: bfloat16 [16, 24576, 2048], P(None, ('sp', 'tp')), may hold values from -6 to 6
- norm_gain: bfloat16 [2048], replicated, may hold values from 0.099609375 to 1.8984375
- key_weight: bfloat16 [2048, 512], replicated, may hold values from -0.125 to 0.125
- value_weight: bfloat16 [2048, 512], replicated, may hold values from -0.125 to 0.125
- query: bfloat16 [16, 1024], P('sp', 'tp'), may hold values from -15 to 15
- head_bias: bfloat16 [16], P('tp'), may hold values from -14 to -6
Outputs:
- key_cache: bfloat16 [16, 24576, 512], P('sp', None, 'tp')
- value_cache: bfloat16 [16, 24576, 512], P('sp', None, 'tp')
- first_read: bfloat16 [16, 1024], P('sp', 'tp')
All inputs are finite; a program needn't handle non-finite values.
Results may differ from a plain program's by a relative error of at most 0.012.
Values may be sent and summed in bfloat16 or wider, within the bound.
No kernel may reach another device: no remote copies, remote signals or barrier semaphores. Data moves between devices by JAX's collectives and lax.ppermute only.
A program may use at most 128 MiB of HBM per device.

v0:
```python
import jax
import jax.numpy as jnp
from jax import lax
from jax.sharding import PartitionSpec as P

HEAD_DIMENSION = 64


EPSILON = 1e-06


def cut_along(value, dim, peers):
    dims = value.shape
    blocks = value.reshape(*dims[:dim], peers, dims[dim] // peers, *dims[dim + 1 :])
    return jnp.moveaxis(blocks, dim, 0)


def in_order(blocks, dim):
    dims = list(blocks.shape[1:])
    dims[dim] *= blocks.shape[0]
    return jnp.moveaxis(blocks, 0, dim).reshape(dims)


def one_exchange(value, axis, axes, splits, concats):
    sizes = [lax.axis_size(a) for a in axes]
    blocks = cut_along(value, splits[0], sizes[0])
    blocks = jnp.moveaxis(cut_along(blocks, splits[1] + 1, sizes[1]), 0, 1)
    inside = blocks.shape[2:]
    blocks = blocks.reshape(-1, *inside)
    blocks = lax.all_to_all(blocks, axis, split_axis=0, concat_axis=0, tiled=True)
    blocks = in_order(blocks.reshape(*sizes, *inside), concats[0] + 1)
    return in_order(blocks, concats[1])


def body(inputs, norm_gain, key_weight, value_weight, query, head_bias):
    groups = lax.axis_size("tp")
    seq_count, span_len, model_width = inputs.shape
    head_cols = key_weight.shape[1] // groups
    kv_heads = head_cols // HEAD_DIMENSION
    q_heads = query.shape[1] // HEAD_DIMENSION
    repeat = q_heads // kv_heads
    widened = inputs.astype(jnp.float32)
    normed = widened * lax.rsqrt(jnp.mean(widened * widened, axis=-1, keepdims=True) + EPSILON)
    normed = (normed * norm_gain.astype(jnp.float32)).astype(jnp.bfloat16)
    key_rows = jnp.einsum(
        "kru,uao->karo",
        normed,
        key_weight.reshape(model_width, groups, head_cols),
        preferred_element_type=jnp.float32,
    ).astype(jnp.bfloat16)
    value_rows = jnp.einsum(
        "kru,uao->karo",
        normed,
        value_weight.reshape(model_width, groups, head_cols),
        preferred_element_type=jnp.float32,
    ).astype(jnp.bfloat16)
    key_cache, value_cache = (
        one_exchange(key_rows, ("tp", "sp"), ("tp", "sp"), (1, 0), (2, 2)),
        one_exchange(value_rows, ("tp", "sp"), ("tp", "sp"), (1, 0), (2, 2)),
    )
    key_cache = key_cache.reshape(1, -1, head_cols)
    value_cache = value_cache.reshape(1, -1, head_cols)
    seq_len = key_cache.shape[1]
    query_tensor = query.reshape(kv_heads, repeat, HEAD_DIMENSION)
    key_tensor = key_cache.reshape(seq_len, kv_heads, HEAD_DIMENSION)
    value_tensor = value_cache.reshape(seq_len, kv_heads, HEAD_DIMENSION)
    score_logits = jnp.einsum(
        "ebx,uex->ebu", query_tensor, key_tensor, preferred_element_type=jnp.float32
    )
    score_logits = score_logits * HEAD_DIMENSION ** (-0.5) + head_bias.astype(jnp.float32).reshape(
        kv_heads, repeat, 1
    )
    log_keep = jax.nn.log_sigmoid(-score_logits)
    suffix_logs = lax.cumsum(log_keep, axis=2, reverse=True) - log_keep
    stick_weights = jnp.exp(jax.nn.log_sigmoid(score_logits) + suffix_logs).astype(jnp.bfloat16)
    attended_output = jnp.einsum(
        "euq,qec->euc", stick_weights, value_tensor, preferred_element_type=jnp.float32
    )
    first_read = attended_output.reshape(1, q_heads * HEAD_DIMENSION).astype(jnp.bfloat16)
    return (key_cache, value_cache, first_read)


def solution(mesh):
    placed = (P(None, ("sp", "tp"), None), P(), P(), P(), P("sp", "tp"), P("tp"))
    return jax.shard_map(
        body,
        mesh=mesh,
        in_specs=placed,
        out_specs=(P("sp", None, "tp"), P("sp", None, "tp"), P("sp", "tp")),
        check_vma=False,
    )
```

profile of v0, /device:TPU:1, one launch (start us, length us, event | category | flops | bytes accessed | tf_op | source)
XLA Modules:
  0.0 168.1 jit_solution(2051911113292594281)
XLA Ops:
  0.7 7.3 %fusion.2 = f32[16,192]{1,0:T(8,128)S(1)} fusion(bf16[16,192,2048]{2,1,0:T(8,128)(2,1)} %param.6), kind=kLoop, calls=%fused_computation.5 | loop fusion | flops 18871296 | bytes 12595200 | tf_op jit(solution)/shard_map/reduce_sum | solution.py:43
  8.0 2.4 %copy.29 = bf16[2048,512]{0,1:T(8,128)(2,1)} copy(bf16[2048,512]{1,0:T(8,128)(2,1)S(1)} %copy-done) | data formatting | bytes 4194304 | tf_op args[2]
  10.3 12.6 %convert_bitcast_fusion.1 = bf16[8,16,1,192,64]{3,4,0,1,2:T(8,128)(2,1)S(1)} fusion(bf16[2048,8,64,1]{0,2,1,3:T(8,128)(2,1)} %bitcast.100, bf16[16,192,2048]{2,1,0:T(8,128)(2,1)} %param.6, f32[2048]{0:T(1024)S(1)} %convert_element_type.43, f32[16,192]{1,0:T(8,128)S(1)} %add_rsqrt_fusion), kind=kOutput, calls=%fused_computation.12 | convolution fusion | flops 6469189632 | bytes 17846272 | tf_op jit(solution)/shard_map/kru,uao->karo/dot_general | solution.py:45
  23.0 2.2 %copy.30 = bf16[8,16,1,192,64]{3,4,1,0,2:T(8,128)(2,1)} copy(bf16[8,16,1,192,64]{3,4,0,1,2:T(8,128)(2,1)S(1)} %convert_bitcast_fusion.1) | data formatting | bytes 6291456 | tf_op jit(solution)/shard_map/transpose | solution.py:15
  25.2 11.9 %all-to-all-start = ((bf16[128,1,1,192,64]{3,4,2,1,0:T(8,128)(2,1)}), bf16[128,1,1,192,64]{3,4,2,1,0:T(8,128)(2,1)}, u32[]{:S(2)}, u32[]{:S(2)}) async-start(bf16[128,1,1,192,64]{3,4,2,1,0:T(8,128)(2,1)} %bitcast.98), calls=%async_computation | async-start | bytes 8388608 | tf_op jit(solution)/shard_map/all_to_all | solution.py:30
  37.2 2.4 %copy.33 = bf16[2048,512]{0,1:T(8,128)(2,1)} copy(bf16[2048,512]{1,0:T(8,128)(2,1)S(1)} %copy-done.1) | data formatting | bytes 4194304 | tf_op args[3]
  39.5 12.6 %convert_bitcast_fusion = bf16[8,16,1,192,64]{3,4,0,1,2:T(8,128)(2,1)S(1)} fusion(bf16[2048,8,64,1]{0,2,1,3:T(8,128)(2,1)} %bitcast.99, bf16[16,192,2048]{2,1,0:T(8,128)(2,1)} %param.6, f32[2048]{0:T(1024)S(1)} %convert_element_type.43, f32[16,192]{1,0:T(8,128)S(1)} %add_rsqrt_fusion), kind=kOutput, calls=%fused_computation.11 | convolution fusion | flops 6469189632 | bytes 17846272 | tf_op jit(solution)/shard_map/kru,uao->karo/dot_general | solution.py:51
  52.1 2.3 %copy.34 = bf16[8,16,1,192,64]{3,4,1,0,2:T(8,128)(2,1)} copy(bf16[8,16,1,192,64]{3,4,0,1,2:T(8,128)(2,1)S(1)} %convert_bitcast_fusion) | data formatting | bytes 6291456 | tf_op jit(solution)/shard_map/transpose | solution.py:15
  54.4 33.4 %all-to-all-done = bf16[128,1,1,192,64]{3,4,2,1,0:T(8,128)(2,1)} async-done(((bf16[128,1,1,192,64]{3,4,2,1,0:T(8,128)(2,1)}), bf16[128,1,1,192,64]{3,4,2,1,0:T(8,128)(2,1)}, u32[]{:S(2)}, u32[]{:S(2)}) %all-to-all-start) | async-done | bytes 3145760 | tf_op jit(solution)/shard_map/all_to_all | solution.py:30
  87.8 6.7 %all-to-all-start.1 = ((bf16[128,1,1,192,64]{3,4,2,1,0:T(8,128)(2,1)}), bf16[128,1,1,192,64]{3,4,2,1,0:T(8,128)(2,1)}, u32[]{:S(2)}, u32[]{:S(2)}) async-start(bf16[128,1,1,192,64]{3,4,2,1,0:T(8,128)(2,1)} %bitcast.97), calls=%async_computation.1 | async-start | bytes 8388608 | tf_op jit(solution)/shard_map/all_to_all | solution.py:30
  94.6 0.5 broadcast.57
  95.1 0.7 reduce.5
  95.9 6.5 %copy.32 = bf16[16,1,1,8,192,64]{4,3,0,5,2,1:T(8,128)(2,1)} copy(bf16[16,1,1,8,192,64]{4,5,0,3,2,1:T(8,128)(2,1)} %bitcast.10) | data formatting | bytes 6291456 | tf_op jit(solution)/shard_map/transpose | solution.py:21
  102.4 6.2 %reshape.155 = bf16[24576,64]{0,1:T(8,128)(2,1)S(1)} reshape(bf16[16,1,1,8,192,64]{4,3,0,5,2,1:T(8,128)(2,1)} %copy.32) | data formatting | bytes 6291456 | tf_op jit(solution)/shard_map/reshape.7
  108.7 7.4 %reshape_reshape_transpose_reshape.6 = bf16[1,24576,64]{1,2,0:T(8,128)(2,1)} reshape(bf16[16,1,1,8,192,64]{4,3,0,5,2,1:T(8,128)(2,1)} %copy.32) | data formatting | bytes 6291456 | tf_op jit(solution)/shard_map/reshape;reshape;transpose;reshape | solution.py:61
  116.1 0.5 fusion.1
  117.2 4.4 %reduce-window.11 = f32[1,2,192,128]{2,3,1,0:T(8,128)S(1)} reduce-window(f32[1,2,192,128]{2,3,1,0:T(8,128)S(1)} %copy.38, f32[]{:T(128)} %constant.12.clone.1), window={size=1x1x1x128 pad=0_0x0_0x0_0x0_127}, to_apply=%region_1.2 | reduce-window | flops 6242304 | bytes 393220 | tf_op jit(solution)/shard_map/reduce-window
  121.8 2.7 %reduce-window.14 = f32[1,2,2,128]{3,2,1,0:T(2,128)S(1)} reduce-window(f32[1,2,2,128]{3,2,1,0:T(2,128)S(1)} %bitcast.103, f32[]{:T(128)} %constant.12.clone.1), window={size=1x1x1x128 pad=0_0x0_0x0_0x0_127}, to_apply=%region_2.3 | reduce-window | flops 65024 | bytes 4100 | tf_op jit(solution)/shard_map/reduce-window.2
  124.6 20.8 %all-to-all-done.1 = bf16[128,1,1,192,64]{3,4,2,1,0:T(8,128)(2,1)} async-done(((bf16[128,1,1,192,64]{3,4,2,1,0:T(8,128)(2,1)}), bf16[128,1,1,192,64]{3,4,2,1,0:T(8,128)(2,1)}, u32[]{:S(2)}, u32[]{:S(2)}) %all-to-all-start.1) | async-done | bytes 3145760 | tf_op jit(solution)/shard_map/all_to_all | solution.py:30
  145.4 6.5 %copy.36 = bf16[16,1,1,8,192,64]{4,3,0,5,2,1:T(8,128)(2,1)} copy(bf16[16,1,1,8,192,64]{4,5,0,3,2,1:T(8,128)(2,1)} %bitcast.20) | data formatting | bytes 6291456 | tf_op jit(solution)/shard_map/transpose | solution.py:21
  151.9 6.2 %reshape.167 = bf16[24576,64]{0,1:T(8,128)(2,1)S(1)} reshape(bf16[16,1,1,8,192,64]{4,3,0,5,2,1:T(8,128)(2,1)} %copy.36) | data formatting | bytes 6291456 | tf_op jit(solution)/shard_map/reshape.25
  158.2 7.4 %reshape_reshape_transpose_reshape.7 = bf16[1,24576,64]{1,2,0:T(8,128)(2,1)} reshape(bf16[16,1,1,8,192,64]{4,3,0,5,2,1:T(8,128)(2,1)} %copy.36) | data formatting | bytes 6291456 | tf_op jit(solution)/shard_map/reshape;reshape;transpose;reshape | solution.py:62
  166.1 1.4 convolution_convert_fusion
  167.5 0.6 convert_element_type.52
  (31 shorter events, 1.5 us)
Async XLA Ops:
  0.6 7.3 %copy-start.2 = (bf16[2048]{0:T(1024)(128)(2,1)S(1)}, bf16[2048]{0:T(1024)(128)(2,1)}, u32[]{:S(2)}) copy-start(bf16[2048]{0:T(1024)(128)(2,1)} %param.7) | copy-start | bytes 12292
  0.6 7.3 %copy-start = (bf16[2048,512]{1,0:T(8,128)(2,1)S(1)}, bf16[2048,512]{1,0:T(8,128)(2,1)}, u32[]{:S(2)}) copy-start(bf16[2048,512]{1,0:T(8,128)(2,1)} %param.8) | copy-start | bytes 6291460
  25.2 12.0 %copy-start.1 = (bf16[2048,512]{1,0:T(8,128)(2,1)S(1)}, bf16[2048,512]{1,0:T(8,128)(2,1)}, u32[]{:S(2)}) copy-start(bf16[2048,512]{1,0:T(8,128)(2,1)} %param.9) | copy-start | bytes 6291460
  25.2 62.7 %all-to-all-start = ((bf16[128,1,1,192,64]{3,4,2,1,0:T(8,128)(2,1)}), bf16[128,1,1,192,64]{3,4,2,1,0:T(8,128)(2,1)}, u32[]{:S(2)}, u32[]{:S(2)}) async-start(bf16[128,1,1,192,64]{3,4,2,1,0:T(8,128)(2,1)} %bitcast.98), calls=%async_computation | async-start | bytes 8388608 | tf_op jit(solution)/shard_map/all_to_all | solution.py:30
  87.8 7.2 %copy-start.3 = (bf16[1,128]{1,0:T(2,128)(2,1)S(1)}, bf16[1,128]{1,0:T(2,128)(2,1)}, u32[]{:S(2)}) copy-start(bf16[1,128]{1,0:T(2,128)(2,1)} %param.10) | copy-start | bytes 772
  87.8 8.0 %copy-start.4 = (bf16[2]{0:T(256)(128)(2,1)S(1)}, bf16[2]{0:T(256)(128)(2,1)}, u32[]{:S(2)}) copy-start(bf16[2]{0:T(256)(128)(2,1)} %param.11) | copy-start | bytes 16
  87.8 8.0 %copy-start.5 = (pred[193]{0:T(512)(128)(4,1)S(1)}, pred[193]{0:T(512)(128)(4,1)}, u32[]{:S(2)}) copy-start(pred[193]{0:T(512)(128)(4,1)} %constant.16.clone.1) | copy-start | bytes 583
  87.8 57.6 %all-to-all-start.1 = ((bf16[128,1,1,192,64]{3,4,2,1,0:T(8,128)(2,1)}), bf16[128,1,1,192,64]{3,4,2,1,0:T(8,128)(2,1)}, u32[]{:S(2)}, u32[]{:S(2)}) async-start(bf16[128,1,1,192,64]{3,4,2,1,0:T(8,128)(2,1)} %bitcast.97), calls=%async_computation.1 | async-start | bytes 8388608 | tf_op jit(solution)/shard_map/all_to_all | solution.py:30
where the time goes:
time: 169 us; the launch traced here: 168 us
  waiting for transfers between devices  54.2 us (32%)
  local copies, waits for them, and re-layouts  51.6 us (31%)
  matrix products  27.1 us (16%)
  starting transfers between devices  18.7 us (11%)
  other arithmetic  15.8 us (9%)
    all_to_all x2, waiting for transfers between devices, one_exchange(): lax.all_to_all(blocks, axis, split_axis=0, concat_axis=0, tiled=True)  54.2 us
    all_to_all x2, starting transfers between devices, one_exchange(): lax.all_to_all(blocks, axis, split_axis=0, concat_axis=0, tiled=True)  18.7 us
    transpose x2, local copies, waits for them, and re-layouts, in_order(): return jnp.moveaxis(blocks, 0, dim).reshape(dims)  13 us
    another operation x11, local copies, waits for them, and re-layouts  13 us
    dot_general x1, matrix products, body(): jnp.einsum('kru,uao->karo', normed, key_weight.reshape(model_width, group...  12.6 us
    dot_general x1, matrix products, body(): jnp.einsum('kru,uao->karo', normed, value_weight.reshape(model_width, gro...  12.6 us
    another operation x1, local copies, waits for them, and re-layouts, body(): key_cache = key_cache.reshape(1, -1, head_cols)  7.43 us
    another operation x1, local copies, waits for them, and re-layouts, body(): value_cache = value_cache.reshape(1, -1, head_cols)  7.43 us
  transfers between devices with their start and end apart: 2, of which 2 were waited for; matrix products, arithmetic and copies ran while one was open for 28% of the time, Pallas kernels for 0%

commit v1 on v0

v1 whole, which is shorter than its diff:
```python
import jax
import jax.numpy as jnp
from jax import lax
from jax.experimental import pallas as pl
from jax.experimental.pallas import tpu as pltpu
from jax.sharding import PartitionSpec as P

HEAD_DIMENSION = 64
EPSILON = 1e-06
LANES = 128


def project_kernel(x_ref, gain_ref, key_ref, value_ref, out_ref, weight_ref, normed_ref):
    seqs, rows, width = x_ref.shape
    groups = out_ref.shape[1]

    @pl.when(pl.program_id(0) == 0)
    def _():
        half = HEAD_DIMENSION
        for pair in range(groups // 2):
            key = key_ref[:, pair * LANES : (pair + 1) * LANES]
            value = value_ref[:, pair * LANES : (pair + 1) * LANES]
            low = jnp.concatenate([key[:, :half], value[:, :half]], axis=1)
            high = jnp.concatenate([key[:, half:], value[:, half:]], axis=1)
            weight_ref[:, 2 * pair * LANES : (2 * pair + 1) * LANES] = low
            weight_ref[:, (2 * pair + 1) * LANES : (2 * pair + 2) * LANES] = high

    gain = gain_ref[...].astype(jnp.float32)
    for s in range(seqs):
        x = x_ref[s].astype(jnp.float32)
        scale = lax.rsqrt(jnp.mean(x * x, axis=-1, keepdims=True) + EPSILON)
        normed_ref[s * rows : (s + 1) * rows, :] = (x * scale * gain).astype(jnp.bfloat16)
    result = jnp.dot(normed_ref[...], weight_ref[...], preferred_element_type=jnp.float32)
    result = result.astype(jnp.bfloat16)
    for s in range(seqs):
        for g in range(groups):
            out_ref[s, g] = result[s * rows : (s + 1) * rows, g * LANES : (g + 1) * LANES]


def project(inputs, gain, key_weight, value_weight, groups, step):
    seqs, rows, width = inputs.shape
    cols = key_weight.shape[1] + value_weight.shape[1]
    return pl.pallas_call(
        project_kernel,
        grid=(seqs // step,),
        in_specs=[
            pl.BlockSpec((step, rows, width), lambda i: (i, 0, 0)),
            pl.BlockSpec((1, width), lambda i: (0, 0)),
            pl.BlockSpec(key_weight.shape, lambda i: (0, 0)),
            pl.BlockSpec(value_weight.shape, lambda i: (0, 0)),
        ],
        out_specs=pl.BlockSpec((step, groups, rows, LANES), lambda i: (i, 0, 0, 0)),
        out_shape=jax.ShapeDtypeStruct((seqs, groups, rows, LANES), jnp.bfloat16),
        scratch_shapes=[
            pltpu.VMEM((width, cols), jnp.bfloat16),
            pltpu.VMEM((step * rows, width), jnp.bfloat16),
        ],
        compiler_params=pltpu.CompilerParams(vmem_limit_bytes=56 * 1024 * 1024),
        name="project",
    )(inputs, gain.reshape(1, width), key_weight, value_weight)


def read_kernel(rows_ref, query_ref, bias_ref, key_ref, value_ref, read_ref, carry_ref, total_ref):
    step = pl.program_id(0)
    sources, span, _ = rows_ref.shape
    count = sources * span
    tiles = count // LANES

    @pl.when(step == 0)
    def _():
        carry_ref[...] = jnp.zeros_like(carry_ref)
        total_ref[...] = jnp.zeros_like(total_ref)

    half = HEAD_DIMENSION
    lane = lax.broadcasted_iota(jnp.int32, (8, LANES), 1)
    row = lax.broadcasted_iota(jnp.int32, (8, LANES), 0)
    query = jnp.broadcast_to(query_ref[...].astype(jnp.float32), (8, LANES))
    swapped = pltpu.roll(query, half, 1)
    heads = jnp.where(row == 0, query, jnp.where(row == 1, swapped, 0.0))
    heads = jnp.where(lane < half, heads, 0.0)
    eye = (
        lax.broadcasted_iota(jnp.int32, (LANES, LANES), 0)
        == lax.broadcasted_iota(jnp.int32, (LANES, LANES), 1)
    ).astype(jnp.float32)
    left = jnp.concatenate([eye, heads], axis=0).astype(jnp.bfloat16)

    block = rows_ref[...].reshape(count, LANES)
    turned = lax.dot_general(left, block, (((1,), (1,)), ((), ())), preferred_element_type=jnp.float32)
    key_ref[...] = turned[:half].astype(jnp.bfloat16)
    value_ref[...] = turned[half:LANES].astype(jnp.bfloat16)

    bias = bias_ref[...].astype(jnp.float32)
    bias = jnp.where(row == 0, bias[:, 0:1], jnp.where(row == 1, bias[:, 1:2], 0.0))
    scores = [
        turned[LANES:, n * LANES : (n + 1) * LANES] * HEAD_DIMENSION ** (-0.5) + bias for n in range(tiles)
    ]
    scores = jnp.concatenate(scores, axis=0)
    soft = jnp.log1p(jnp.exp(-jnp.abs(scores)))
    keep = jnp.minimum(-scores, 0.0) - soft
    take = jnp.minimum(scores, 0.0) - soft
    later = lax.broadcasted_iota(jnp.int32, (LANES, 2 * LANES), 0)
    here = lax.broadcasted_iota(jnp.int32, (LANES, 2 * LANES), 1)
    sums_of = jnp.where((later > here) | (here >= LANES), 1.0, 0.0)
    sums = jnp.dot(keep, sums_of, preferred_element_type=jnp.float32, precision=lax.Precision.HIGHEST)
    carry = carry_ref[...]
    suffixes = [None] * tiles
    for n in reversed(range(tiles)):
        suffixes[n] = sums[8 * n : 8 * n + 8, :LANES] + carry
        carry = carry + sums[8 * n : 8 * n + 8, LANES:]
    carry_ref[...] = carry
    weights = jnp.exp(take + jnp.concatenate(suffixes, axis=0)).astype(jnp.bfloat16)
    weights = jnp.concatenate([weights[8 * n : 8 * n + 8] for n in range(tiles)], axis=1)
    total_ref[...] += jnp.dot(weights, block, preferred_element_type=jnp.float32)

    @pl.when(step == pl.num_programs(0) - 1)
    def _():
        total = total_ref[...]
        first = pltpu.roll(total, half, 1)[0:1]
        read_ref[...] = jnp.where(lane[0:1] < half, first, total[1:2]).astype(jnp.bfloat16)


def read(received, query, bias, step):
    sources, span, _ = received.shape
    steps = sources // step
    length = sources * span
    key, value, first = pl.pallas_call(
        read_kernel,
        grid=(steps,),
        in_specs=[
            pl.BlockSpec((step, span, LANES), lambda i: (steps - 1 - i, 0, 0)),
            pl.BlockSpec((1, LANES), lambda i: (0, 0)),
            pl.BlockSpec((1, 2), lambda i: (0, 0)),
        ],
        out_specs=[
            pl.BlockSpec((HEAD_DIMENSION, step * span), lambda i: (0, steps - 1 - i)),
            pl.BlockSpec((HEAD_DIMENSION, step * span), lambda i: (0, steps - 1 - i)),
            pl.BlockSpec((1, LANES), lambda i: (0, 0)),
        ],
        out_shape=[
            jax.ShapeDtypeStruct((HEAD_DIMENSION, length), jnp.bfloat16),
            jax.ShapeDtypeStruct((HEAD_DIMENSION, length), jnp.bfloat16),
            jax.ShapeDtypeStruct((1, LANES), jnp.bfloat16),
        ],
        scratch_shapes=[pltpu.VMEM((8, LANES), jnp.float32), pltpu.VMEM((8, LANES), jnp.float32)],
        compiler_params=pltpu.CompilerParams(vmem_limit_bytes=48 * 1024 * 1024),
        name="read",
    )(received, query, bias.reshape(1, 2))
    return key.T[None], value.T[None], first


def body(inputs, norm_gain, key_weight, value_weight, query, head_bias):
    groups = lax.axis_size("tp")
    peers = lax.axis_size("sp") * groups
    span = inputs.shape[1]
    sent = project(inputs, norm_gain, key_weight, value_weight, groups, 4)
    sent = sent.reshape(peers, span, LANES)
    received = lax.all_to_all(sent, ("sp", "tp"), split_axis=0, concat_axis=0, tiled=True)
    return read(received, query, head_bias, 16)


def solution(mesh):
    placed = (P(None, ("sp", "tp"), None), P(), P(), P(), P("sp", "tp"), P("tp"))
    return jax.shard_map(
        body,
        mesh=mesh,
        in_specs=placed,
        out_specs=(P("sp", None, "tp"), P("sp", None, "tp"), P("sp", "tp")),
        check_vma=False,
    )
```

time: 169 us -> 122 us (0.72)
  blocking collectives: 0 us -> 87 us
  waiting for transfers between devices: 54.2 us -> 0 us
  local copies, waits for them, and re-layouts: 51.6 us -> 1.3 us
  Pallas kernels: 0 us -> 33 us
  matrix products: 27.1 us -> 0 us
  starting transfers between devices: 18.7 us -> 0 us
  other arithmetic: 15.8 us -> 0 us
    all_to_all x0 -> x1, blocking collectives: none -> 87 us  [body(): lax.all_to_all(sent, ('sp', 'tp'), split_axis=0, concat_axis=0, tiled=True)]
    all_to_all x2 -> x0, waiting for transfers between devices: 54.2 us -> none  [one_exchange(): lax.all_to_all(blocks, axis, split_axis=0, concat_axis=0, tiled=True)]
    pallas_call x0 -> x2, Pallas kernels: none -> 33 us  [the longest x1 21.9 us: project(): pl.pallas_call(project_kernel, grid=(seqs // step,), in_specs=[pl.BlockSp...]
    another operation x13 -> x0, local copies, waits for them, and re-layouts: 27.9 us -> none
    dot_general x4 -> x0, matrix products: 27.1 us -> none  [the longest x1 12.6 us: body(): jnp.einsum('kru,uao->karo', normed, key_weight.reshape(model_width, group...]
    all_to_all x2 -> x0, starting transfers between devices: 18.7 us -> none  [one_exchange(): lax.all_to_all(blocks, axis, split_axis=0, concat_axis=0, tiled=True)]
    transpose x4 -> x0, local copies, waits for them, and re-layouts: 17.6 us -> none  [the longest x2 13 us: in_order(): return jnp.moveaxis(blocks, 0, dim).reshape(dims)]
    another operation x4 -> x0, other arithmetic: 7.39 us -> none
  transfers between devices with their start and end apart: 2 -> 0, of which waited for: 2 -> 0; matrix products, arithmetic and copies ran while one was open for 28% -> 0% of each run, Pallas kernels for 0% -> 0%
where the time goes in v1:
time: 122 us
  blocking collectives  87 us (71%)
  Pallas kernels  33 us (27%)
  local copies, waits for them, and re-layouts  1.3 us (1%)
    all_to_all x1, blocking collectives, body(): lax.all_to_all(sent, ('sp', 'tp'), split_axis=0, concat_axis=0, tiled=True)  87 us
    pallas_call x1, Pallas kernels, project(): pl.pallas_call(project_kernel, grid=(seqs // step,), in_specs=[pl.BlockSp...  21.9 us
    pallas_call x1, Pallas kernels, read(): pl.pallas_call(read_kernel, grid=(steps,), in_specs=[pl.BlockSpec((step,...  11.1 us

profile of v1, /device:TPU:1, one launch (start us, length us, event | category | flops | bytes accessed | tf_op | source)
XLA Modules:
  0.0 121.9 jit_solution(6437905892086841257)
XLA Ops:
  0.6 1.3 %reshape.15.gain_ref = bf16[1,2048]{1,0:T(2,128)(2,1)} reshape(bf16[2048]{0:T(1024)(128)(2,1)} %param.7) | data formatting | bytes 8192 | tf_op jit(solution)/shard_map/reshape | solution.py:60
  1.9 21.9 %project.1 = bf16[16,8,192,128]{3,2,1,0:T(8,128)(2,1)} custom-call(bf16[16,192,2048]{2,1,0:T(8,128)(2,1)} %x_ref.1, bf16[1,2048]{1,0:T(2,128)(2,1)} %reshape.15.gain_ref, bf16[2048,512]{1,0:T(8,128)(2,1)} %key_ref.1, bf16[2048,512]{1,0:T(8,128)(2,1)} %value_ref.1), custom_call_target="tpu_custom_call" | custom-call | tf_op jit(solution)/shard_map/project/pallas_call | solution.py:43
  23.8 0.0 copy-start
  23.8 0.0 copy-start.1
  23.8 87.0 %all_to_all.5.rows_ref = bf16[128,192,128]{2,1,0:T(8,128)(2,1)} all-to-all(bf16[128,192,128]{2,1,0:T(8,128)(2,1)} %bitcast.9), channel_id=1, replica_groups=mesh['sp'=16,'tp'=8] {'sp','tp'}, dimensions={0} | all-to-all | bytes 12582912 | tf_op jit(solution)/shard_map/all_to_all | solution.py:157
  110.8 0.0 copy-done
  110.8 0.0 copy-done.1
  110.8 11.1 %read.1 = (bf16[64,24576]{1,0:T(8,128)(2,1)}, bf16[64,24576]{1,0:T(8,128)(2,1)}, bf16[1,128]{1,0:T(2,128)(2,1)}) custom-call(bf16[128,192,128]{2,1,0:T(8,128)(2,1)} %all_to_all.5.rows_ref, bf16[1,128]{1,0:T(2,128)(2,1)S(1)} %copy-done, bf16[1,2]{1,0:T(2,128)(2,1)S(1)} %bitcast.8), custom_call_target="tpu_custom_call" | custom-call | tf_op jit(solution)/shard_map/read/pallas_call | solution.py:126
Async XLA Ops:
  23.8 87.0 %copy-start = (bf16[1,128]{1,0:T(2,128)(2,1)S(1)}, bf16[1,128]{1,0:T(2,128)(2,1)}, u32[]{:S(2)}) copy-start(bf16[1,128]{1,0:T(2,128)(2,1)} %query_ref.1) | copy-start | bytes 772
  23.8 87.0 %copy-start.1 = (bf16[2]{0:T(256)(128)(2,1)S(1)}, bf16[2]{0:T(256)(128)(2,1)}, u32[]{:S(2)}) copy-start(bf16[2]{0:T(256)(128)(2,1)} %param.11) | copy-start | bytes 16

commit v2 on v1

v2 whole, which is shorter than its diff:
```python
import jax
import jax.numpy as jnp
from jax import lax
from jax.experimental import pallas as pl
from jax.experimental.pallas import tpu as pltpu
from jax.sharding import PartitionSpec as P

HEAD_DIMENSION = 64
EPSILON = 1e-06
LANES = 128


def project_kernel(x_ref, gain_ref, key_ref, value_ref, out_ref, normed_ref):
    seqs, rows, width = x_ref.shape
    groups = out_ref.shape[1]
    half = HEAD_DIMENSION
    odd = lax.axis_index("tp") & 1
    gain = gain_ref[...].astype(jnp.float32).reshape(1, width)

    def normalize(s, start, count, to):
        x = x_ref[s, pl.ds(start, count), :].astype(jnp.float32)
        scale = lax.rsqrt(jnp.mean(x * x, axis=-1, keepdims=True) + EPSILON)
        normed_ref[to : to + count, :] = (x * scale * gain).astype(jnp.bfloat16)

    for s in range(seqs):
        normalize(s, pl.multiple_of(odd * half, half), LANES, s * LANES)
        normalize(s, pl.multiple_of((1 - odd) * LANES, half), half, seqs * LANES + s * half)
    contract = (((0,), (1,)), ((), ()))
    keys = lax.dot_general(key_ref[...], normed_ref[...], contract, preferred_element_type=jnp.float32)
    values = lax.dot_general(value_ref[...], normed_ref[...], contract, preferred_element_type=jnp.float32)
    low = lax.broadcasted_iota(jnp.int32, (half, LANES), 1) < half
    for s in range(seqs):
        lanes = slice(s * LANES, (s + 1) * LANES)
        rest = slice((seqs + s // 2) * LANES, (seqs + s // 2 + 1) * LANES)
        for g in range(groups):
            heads = slice(g * half, (g + 1) * half)
            out_ref[s, g, :half] = keys[heads, lanes].astype(jnp.bfloat16)
            out_ref[s, g, half:LANES] = values[heads, lanes].astype(jnp.bfloat16)
            first = jnp.where(odd == 0, keys[heads, rest], values[heads, rest])
            second = jnp.where(odd == 0, values[heads, rest], keys[heads, rest])
            if s % 2 == 0:
                second = pltpu.roll(second, half, 1)
            else:
                first = pltpu.roll(first, half, 1)
            out_ref[s, g, LANES:] = jnp.where(low, first, second).astype(jnp.bfloat16)


def project(inputs, gain, key_weight, value_weight, groups, step):
    seqs, rows, width = inputs.shape
    return pl.pallas_call(
        project_kernel,
        grid=(seqs // step,),
        in_specs=[
            pl.BlockSpec((step, rows, width), lambda i: (i, 0, 0)),
            pl.BlockSpec((width,), lambda i: (0,)),
            pl.BlockSpec(key_weight.shape, lambda i: (0, 0)),
            pl.BlockSpec(value_weight.shape, lambda i: (0, 0)),
        ],
        out_specs=pl.BlockSpec((step, groups, rows, LANES), lambda i: (i, 0, 0, 0)),
        out_shape=jax.ShapeDtypeStruct((seqs, groups, rows, LANES), jnp.bfloat16),
        scratch_shapes=[pltpu.VMEM((step * rows, width), jnp.bfloat16)],
        compiler_params=pltpu.CompilerParams(vmem_limit_bytes=56 * 1024 * 1024),
        name="project",
    )(inputs, gain, key_weight, value_weight)


def read_kernel(rows_ref, query_ref, bias_ref, key_ref, value_ref, read_ref, carry_ref, total_ref):
    step = pl.program_id(0)
    sources, span, _ = rows_ref.shape
    tiles = sources * span // LANES
    half = HEAD_DIMENSION

    @pl.when(step == 0)
    def _():
        carry_ref[...] = jnp.zeros_like(carry_ref)
        total_ref[...] = jnp.zeros_like(total_ref)

    low = lax.broadcasted_iota(jnp.int32, (half, LANES), 1) < half
    for pair in range(sources // 2):
        even = rows_ref[2 * pair]
        odd = rows_ref[2 * pair + 1]
        at = 3 * LANES * pair
        key_ref[:, at : at + LANES] = even[:half]
        value_ref[:, at : at + LANES] = even[half:LANES]
        first = even[LANES:].astype(jnp.float32)
        second = odd[LANES:].astype(jnp.float32)
        key_ref[:, at + LANES : at + 2 * LANES] = jnp.where(low, first, second).astype(jnp.bfloat16)
        middle = pltpu.roll(jnp.where(low, second, first), half, 1)
        value_ref[:, at + LANES : at + 2 * LANES] = middle.astype(jnp.bfloat16)
        key_ref[:, at + 2 * LANES : at + 3 * LANES] = odd[:half]
        value_ref[:, at + 2 * LANES : at + 3 * LANES] = odd[half:LANES]

    row = lax.broadcasted_iota(jnp.int32, (8, LANES), 0)
    query = jnp.broadcast_to(query_ref[...].astype(jnp.float32), (8, LANES))
    query = jnp.where(row == 0, query, jnp.where(row == 1, pltpu.roll(query, half, 1), 0.0))
    query = query[:, :half].astype(jnp.bfloat16)
    logits = jnp.dot(query, key_ref[...], preferred_element_type=jnp.float32)
    bias = bias_ref[...].astype(jnp.float32)
    bias = jnp.where(row == 0, bias[:, 0:1], jnp.where(row == 1, bias[:, 1:2], 0.0))
    scores = [logits[:, n * LANES : (n + 1) * LANES] * HEAD_DIMENSION ** (-0.5) + bias for n in range(tiles)]
    scores = jnp.concatenate(scores, axis=0)
    soft = jnp.log1p(jnp.exp(-jnp.abs(scores)))
    keep = jnp.minimum(-scores, 0.0) - soft
    take = jnp.minimum(scores, 0.0) - soft
    later = lax.broadcasted_iota(jnp.int32, (LANES, 2 * LANES), 0)
    here = lax.broadcasted_iota(jnp.int32, (LANES, 2 * LANES), 1)
    sums_of = jnp.where((later > here) | (here >= LANES), 1.0, 0.0)
    sums = jnp.dot(keep, sums_of, preferred_element_type=jnp.float32, precision=lax.Precision.HIGHEST)
    carry = carry_ref[...]
    suffixes = [None] * tiles
    for n in reversed(range(tiles)):
        suffixes[n] = sums[8 * n : 8 * n + 8, :LANES] + carry
        carry = carry + sums[8 * n : 8 * n + 8, LANES:]
    carry_ref[...] = carry
    weights = jnp.exp(take + jnp.concatenate(suffixes, axis=0)).astype(jnp.bfloat16)
    weights = jnp.concatenate([weights[8 * n : 8 * n + 8] for n in range(tiles)], axis=1)
    total_ref[...] += lax.dot_general(
        weights, value_ref[...], (((1,), (1,)), ((), ())), preferred_element_type=jnp.float32
    )

    @pl.when(step == pl.num_programs(0) - 1)
    def _():
        read_ref[:, :half] = total_ref[0:1].astype(jnp.bfloat16)
        read_ref[:, half:] = total_ref[1:2].astype(jnp.bfloat16)


def read(received, query, bias, step):
    sources, span, _ = received.shape
    steps = sources // step
    length = sources * span
    key, value, first = pl.pallas_call(
        read_kernel,
        grid=(steps,),
        in_specs=[
            pl.BlockSpec((step, span, LANES), lambda i: (steps - 1 - i, 0, 0)),
            pl.BlockSpec((1, LANES), lambda i: (0, 0)),
            pl.BlockSpec((1, 2), lambda i: (0, 0)),
        ],
        out_specs=[
            pl.BlockSpec((HEAD_DIMENSION, step * span), lambda i: (0, steps - 1 - i)),
            pl.BlockSpec((HEAD_DIMENSION, step * span), lambda i: (0, steps - 1 - i)),
            pl.BlockSpec((1, LANES), lambda i: (0, 0)),
        ],
        out_shape=[
            jax.ShapeDtypeStruct((HEAD_DIMENSION, length), jnp.bfloat16),
            jax.ShapeDtypeStruct((HEAD_DIMENSION, length), jnp.bfloat16),
            jax.ShapeDtypeStruct((1, LANES), jnp.bfloat16),
        ],
        scratch_shapes=[pltpu.VMEM((8, LANES), jnp.float32), pltpu.VMEM((8, HEAD_DIMENSION), jnp.float32)],
        compiler_params=pltpu.CompilerParams(vmem_limit_bytes=24 * 1024 * 1024),
        name="read",
    )(received, query, bias.reshape(1, 2))
    return key.T[None], value.T[None], first


def body(inputs, norm_gain, key_weight, value_weight, query, head_bias):
    groups = lax.axis_size("tp")
    peers = lax.axis_size("sp") * groups
    span = inputs.shape[1]
    sent = project(inputs, norm_gain, key_weight, value_weight, groups, 4)
    sent = sent.reshape(peers, span, LANES)
    received = lax.all_to_all(sent, ("sp", "tp"), split_axis=0, concat_axis=0, tiled=True)
    return read(received, query, head_bias, 32)


def solution(mesh):
    placed = (P(None, ("sp", "tp"), None), P(), P(), P(), P("sp", "tp"), P("tp"))
    return jax.shard_map(
        body,
        mesh=mesh,
        in_specs=placed,
        out_specs=(P("sp", None, "tp"), P("sp", None, "tp"), P("sp", "tp")),
        check_vma=False,
    )
```

time: 122 us -> 114 us (0.934)
  Pallas kernels: 33 us -> 26.2 us
  local copies, waits for them, and re-layouts: 1.3 us -> 0.01 us
    pallas_call x1, Pallas kernels: 11.1 us -> 5.82 us  [read(): pl.pallas_call(read_kernel, grid=(steps,), in_specs=[pl.BlockSpec((step,...]
    pallas_call x1, Pallas kernels: 21.9 us -> 20.4 us  [project(): pl.pallas_call(project_kernel, grid=(seqs // step,), in_specs=[pl.BlockSp...]
    reshape x1 -> x0, local copies, waits for them, and re-layouts: 1.29 us -> none  [project(): gain.reshape(1, width)]
where the time goes in v2:
time: 114 us
  blocking collectives  86.9 us (76%)
  Pallas kernels  26.2 us (23%)
    all_to_all x1, blocking collectives, body(): lax.all_to_all(sent, ('sp', 'tp'), split_axis=0, concat_axis=0, tiled=True)  86.9 us
    pallas_call x1, Pallas kernels, project(): pl.pallas_call(project_kernel, grid=(seqs // step,), in_specs=[pl.BlockSp...  20.4 us
    pallas_call x1, Pallas kernels, read(): pl.pallas_call(read_kernel, grid=(steps,), in_specs=[pl.BlockSpec((step,...  5.82 us

profile of v2, /device:TPU:1, one launch (start us, length us, event | category | flops | bytes accessed | tf_op | source)
XLA Modules:
  0.0 113.8 jit_solution(11431342938067989254)
XLA Ops:
  0.6 20.4 %project.1 = bf16[16,8,192,128]{3,2,1,0:T(8,128)(2,1)} custom-call(bf16[16,192,2048]{2,1,0:T(8,128)(2,1)} %x_ref.1, bf16[2048]{0:T(1024)(128)(2,1)} %gain_ref.1, bf16[2048,512]{1,0:T(8,128)(2,1)} %key_ref.1, bf16[2048,512]{1,0:T(8,128)(2,1)} %value_ref.1), custom_call_target="tpu_custom_call" | custom-call | tf_op jit(solution)/shard_map/project/pallas_call | solution.py:50
  21.0 0.0 copy-start
  21.0 0.0 copy-start.1
  21.0 86.9 %all_to_all.5.rows_ref = bf16[128,192,128]{2,1,0:T(8,128)(2,1)S(1)} all-to-all(bf16[128,192,128]{2,1,0:T(8,128)(2,1)} %bitcast.9), channel_id=1, replica_groups=mesh['sp'=16,'tp'=8] {'sp','tp'}, dimensions={0} | all-to-all | bytes 12582912 | tf_op jit(solution)/shard_map/all_to_all | solution.py:162
  107.9 0.0 copy-done
  107.9 0.0 copy-done.1
  108.0 5.8 %read.1 = (bf16[64,24576]{1,0:T(8,128)(2,1)}, bf16[64,24576]{1,0:T(8,128)(2,1)}, bf16[1,128]{1,0:T(2,128)(2,1)}) custom-call(bf16[128,192,128]{2,1,0:T(8,128)(2,1)S(1)} %all_to_all.5.rows_ref, bf16[1,128]{1,0:T(2,128)(2,1)S(1)} %copy-done, bf16[1,2]{1,0:T(2,128)(2,1)S(1)} %bitcast.8), custom_call_target="tpu_custom_call" | custom-call | tf_op jit(solution)/shard_map/read/pallas_call | solution.py:131
Async XLA Ops:
  21.0 86.9 %copy-start = (bf16[1,128]{1,0:T(2,128)(2,1)S(1)}, bf16[1,128]{1,0:T(2,128)(2,1)}, u32[]{:S(2)}) copy-start(bf16[1,128]{1,0:T(2,128)(2,1)} %query_ref.1) | copy-start | bytes 772
  21.0 86.9 %copy-start.1 = (bf16[2]{0:T(256)(128)(2,1)S(1)}, bf16[2]{0:T(256)(128)(2,1)}, u32[]{:S(2)}) copy-start(bf16[2]{0:T(256)(128)(2,1)} %param.11) | copy-start | bytes 16

commit v3 on v2

--- a/solution.py
+++ b/solution.py
@@ -24,6 +24,7 @@
 
     for s in range(seqs):
         normalize(s, pl.multiple_of(odd * half, half), LANES, s * LANES)
+    for s in range(seqs):
         normalize(s, pl.multiple_of((1 - odd) * LANES, half), half, seqs * LANES + s * half)
     contract = (((0,), (1,)), ((), ()))
     keys = lax.dot_general(key_ref[...], normed_ref[...], contract, preferred_element_type=jnp.float32)
@@ -105,12 +106,28 @@
     later = lax.broadcasted_iota(jnp.int32, (LANES, 2 * LANES), 0)
     here = lax.broadcasted_iota(jnp.int32, (LANES, 2 * LANES), 1)
     sums_of = jnp.where((later > here) | (here >= LANES), 1.0, 0.0)
-    sums = jnp.dot(keep, sums_of, preferred_element_type=jnp.float32, precision=lax.Precision.HIGHEST)
+    sums_of = sums_of.astype(jnp.bfloat16)
+    pieces = []
+    for _ in range(3):
+        pieces.append(keep.astype(jnp.bfloat16))
+        keep = keep - pieces[-1].astype(jnp.float32)
+    sums = jnp.dot(
+        jnp.concatenate(pieces, axis=1),
+        jnp.concatenate([sums_of] * 3, axis=0),
+        preferred_element_type=jnp.float32,
+    )
     carry = carry_ref[...]
     suffixes = [None] * tiles
-    for n in reversed(range(tiles)):
-        suffixes[n] = sums[8 * n : 8 * n + 8, :LANES] + carry
-        carry = carry + sums[8 * n : 8 * n + 8, LANES:]
+    for top in reversed(range(0, tiles, 8)):
+        later_tiles = None
+        for n in reversed(range(top, top + 8)):
+            own = sums[8 * n : 8 * n + 8, :LANES]
+            suffixes[n] = own if later_tiles is None else own + later_tiles
+            whole = sums[8 * n : 8 * n + 8, LANES:]
+            later_tiles = whole if later_tiles is None else later_tiles + whole
+        for n in range(top, top + 8):
+            suffixes[n] = suffixes[n] + carry
+        carry = carry + later_tiles
     carry_ref[...] = carry
     weights = jnp.exp(take + jnp.concatenate(suffixes, axis=0)).astype(jnp.bfloat16)
     weights = jnp.concatenate([weights[8 * n : 8 * n + 8] for n in range(tiles)], axis=1)
@@ -147,7 +164,7 @@
             jax.ShapeDtypeStruct((1, LANES), jnp.bfloat16),
         ],
         scratch_shapes=[pltpu.VMEM((8, LANES), jnp.float32), pltpu.VMEM((8, HEAD_DIMENSION), jnp.float32)],
-        compiler_params=pltpu.CompilerParams(vmem_limit_bytes=24 * 1024 * 1024),
+        compiler_params=pltpu.CompilerParams(vmem_limit_bytes=36 * 1024 * 1024),
         name="read",
     )(received, query, bias.reshape(1, 2))
     return key.T[None], value.T[None], first
@@ -160,7 +177,7 @@
     sent = project(inputs, norm_gain, key_weight, value_weight, groups, 4)
     sent = sent.reshape(peers, span, LANES)
     received = lax.all_to_all(sent, ("sp", "tp"), split_axis=0, concat_axis=0, tiled=True)
-    return read(received, query, head_bias, 32)
+    return read(received, query, head_bias, 64)
 
 
 def solution(mesh):

time: 114 us -> 113 us (level)
  no operation moved by 1% of the time
where the time goes in v3:
time: 113 us
  blocking collectives  86.9 us (77%)
  Pallas kernels  25.8 us (23%)
    all_to_all x1, blocking collectives, body(): lax.all_to_all(sent, ('sp', 'tp'), split_axis=0, concat_axis=0, tiled=True)  86.9 us
    pallas_call x1, Pallas kernels, project(): pl.pallas_call(project_kernel, grid=(seqs // step,), in_specs=[pl.BlockSp...  20.4 us
    pallas_call x1, Pallas kernels, read(): pl.pallas_call(read_kernel, grid=(steps,), in_specs=[pl.BlockSpec((step,...  5.34 us

profile of v3, /device:TPU:1, one launch (start us, length us, event | category | flops | bytes accessed | tf_op | source)
XLA Modules:
  0.0 113.3 jit_solution(15000006363102192162)
XLA Ops:
  0.6 20.4 %project.1 = bf16[16,8,192,128]{3,2,1,0:T(8,128)(2,1)} custom-call(bf16[16,192,2048]{2,1,0:T(8,128)(2,1)} %x_ref.1, bf16[2048]{0:T(1024)(128)(2,1)} %gain_ref.1, bf16[2048,512]{1,0:T(8,128)(2,1)} %key_ref.1, bf16[2048,512]{1,0:T(8,128)(2,1)} %value_ref.1), custom_call_target="tpu_custom_call" | custom-call | tf_op jit(solution)/shard_map/project/pallas_call | solution.py:51
  21.0 0.0 copy-start
  21.0 0.0 copy-start.1
  21.0 86.9 %all_to_all.5.rows_ref = bf16[128,192,128]{2,1,0:T(8,128)(2,1)S(1)} all-to-all(bf16[128,192,128]{2,1,0:T(8,128)(2,1)} %bitcast.9), channel_id=1, replica_groups=mesh['sp'=16,'tp'=8] {'sp','tp'}, dimensions={0} | all-to-all | bytes 12582912 | tf_op jit(solution)/shard_map/all_to_all | solution.py:179
  107.9 0.0 copy-done
  107.9 0.0 copy-done.1
  108.0 5.3 %read.1 = (bf16[64,24576]{1,0:T(8,128)(2,1)}, bf16[64,24576]{1,0:T(8,128)(2,1)}, bf16[1,128]{1,0:T(2,128)(2,1)}) custom-call(bf16[128,192,128]{2,1,0:T(8,128)(2,1)S(1)} %all_to_all.5.rows_ref, bf16[1,128]{1,0:T(2,128)(2,1)S(1)} %copy-done, bf16[1,2]{1,0:T(2,128)(2,1)S(1)} %bitcast.8), custom_call_target="tpu_custom_call" | custom-call | tf_op jit(solution)/shard_map/read/pallas_call | solution.py:148
Async XLA Ops:
  21.0 86.9 %copy-start = (bf16[1,128]{1,0:T(2,128)(2,1)S(1)}, bf16[1,128]{1,0:T(2,128)(2,1)}, u32[]{:S(2)}) copy-start(bf16[1,128]{1,0:T(2,128)(2,1)} %query_ref.1) | copy-start | bytes 772
  21.0 86.9 %copy-start.1 = (bf16[2]{0:T(256)(128)(2,1)S(1)}, bf16[2]{0:T(256)(128)(2,1)}, u32[]{:S(2)}) copy-start(bf16[2]{0:T(256)(128)(2,1)} %param.11) | copy-start | bytes 16

commit v4 on v3

--- a/solution.py
+++ b/solution.py
@@ -83,10 +83,10 @@
         at = 3 * LANES * pair
         key_ref[:, at : at + LANES] = even[:half]
         value_ref[:, at : at + LANES] = even[half:LANES]
-        first = even[LANES:].astype(jnp.float32)
-        second = odd[LANES:].astype(jnp.float32)
-        key_ref[:, at + LANES : at + 2 * LANES] = jnp.where(low, first, second).astype(jnp.bfloat16)
-        middle = pltpu.roll(jnp.where(low, second, first), half, 1)
+        first = even[LANES:]
+        second = odd[LANES:]
+        key_ref[:, at + LANES : at + 2 * LANES] = jnp.where(low, first, second)
+        middle = pltpu.roll(jnp.where(low, second, first).astype(jnp.float32), half, 1)
         value_ref[:, at + LANES : at + 2 * LANES] = middle.astype(jnp.bfloat16)
         key_ref[:, at + 2 * LANES : at + 3 * LANES] = odd[:half]
         value_ref[:, at + 2 * LANES : at + 3 * LANES] = odd[half:LANES]

time: 113 us -> 114 us (level)
  no operation moved by 1% of the time
where the time goes in v4:
time: 114 us; the launch traced here: 113 us
  blocking collectives  86.9 us (76%)
  Pallas kernels  25.8 us (23%)
    all_to_all x1, blocking collectives, body(): lax.all_to_all(sent, ('sp', 'tp'), split_axis=0, concat_axis=0, tiled=True)  86.9 us
    pallas_call x1, Pallas kernels, project(): pl.pallas_call(project_kernel, grid=(seqs // step,), in_specs=[pl.BlockSp...  20.4 us
    pallas_call x1, Pallas kernels, read(): pl.pallas_call(read_kernel, grid=(steps,), in_specs=[pl.BlockSpec((step,...  5.38 us

profile of v4, /device:TPU:1, one launch (start us, length us, event | category | flops | bytes accessed | tf_op | source)
XLA Modules:
  0.0 113.3 jit_solution(1207465342865177010)
XLA Ops:
  0.6 20.4 %project.1 = bf16[16,8,192,128]{3,2,1,0:T(8,128)(2,1)} custom-call(bf16[16,192,2048]{2,1,0:T(8,128)(2,1)} %x_ref.1, bf16[2048]{0:T(1024)(128)(2,1)} %gain_ref.1, bf16[2048,512]{1,0:T(8,128)(2,1)} %key_ref.1, bf16[2048,512]{1,0:T(8,128)(2,1)} %value_ref.1), custom_call_target="tpu_custom_call" | custom-call | tf_op jit(solution)/shard_map/project/pallas_call | solution.py:51
  21.0 0.0 copy-start
  21.0 0.0 copy-start.1
  21.0 86.9 %all_to_all.5.rows_ref = bf16[128,192,128]{2,1,0:T(8,128)(2,1)S(1)} all-to-all(bf16[128,192,128]{2,1,0:T(8,128)(2,1)} %bitcast.9), channel_id=1, replica_groups=mesh['sp'=16,'tp'=8] {'sp','tp'}, dimensions={0} | all-to-all | bytes 12582912 | tf_op jit(solution)/shard_map/all_to_all | solution.py:179
  107.9 0.0 copy-done
  107.9 0.0 copy-done.1
  108.0 5.4 %read.1 = (bf16[64,24576]{1,0:T(8,128)(2,1)}, bf16[64,24576]{1,0:T(8,128)(2,1)}, bf16[1,128]{1,0:T(2,128)(2,1)}) custom-call(bf16[128,192,128]{2,1,0:T(8,128)(2,1)S(1)} %all_to_all.5.rows_ref, bf16[1,128]{1,0:T(2,128)(2,1)S(1)} %copy-done, bf16[1,2]{1,0:T(2,128)(2,1)S(1)} %bitcast.8), custom_call_target="tpu_custom_call" | custom-call | tf_op jit(solution)/shard_map/read/pallas_call | solution.py:148
Async XLA Ops:
  21.0 86.9 %copy-start = (bf16[1,128]{1,0:T(2,128)(2,1)S(1)}, bf16[1,128]{1,0:T(2,128)(2,1)}, u32[]{:S(2)}) copy-start(bf16[1,128]{1,0:T(2,128)(2,1)} %query_ref.1) | copy-start | bytes 772
  21.0 86.9 %copy-start.1 = (bf16[2]{0:T(256)(128)(2,1)S(1)}, bf16[2]{0:T(256)(128)(2,1)}, u32[]{:S(2)}) copy-start(bf16[2]{0:T(256)(128)(2,1)} %param.11) | copy-start | bytes 16
